TPU v7x, 32 devices: a whole 2x2x4 slice. The times are simulated.
32 devices in a mesh: ep: 8 (over z, x), tp: 4 (over y, core).
Axes of the slice: x: 2, y: 2, z: 4, core: 2. Of those that a mesh axis runs over, the one named last changes fastest.
Arguments:
- hidden_in: bfloat16 [256, 2048], P('ep', 'tp'), may hold values from -6 to 6
- state_in: float32 [256, 8, 128, 128], P('ep', 'tp'), may hold values from -0.6 to 0.6
- attn_gain: float32 [2048], replicated, may hold values from 0.1 to 1.9
- w_query: bfloat16 [2048, 1024], P(None, 'tp'), may hold values from -0.125 to 0.125
- w_key: bfloat16 [2048, 1024], P(None, 'tp'), may hold values from -0.125 to 0.125
- w_value: bfloat16 [2048, 1024], P(None, 'tp'), may hold values from -0.125 to 0.125
- w_gate: bfloat16 [2048, 1024], P(None, 'tp'), may hold values from -0.125 to 0.125
- w_beta: bfloat16 [2048, 8], replicated, may hold values from -0.125 to 0.125
- w_decay: bfloat16 [2048, 8], replicated, may hold values from -0.125 to 0.125
- decay_scale: float32 [8], replicated, may hold values from 0.05 to 3
- head_gain: float32 [128], replicated, may hold values from 0.1 to 1.9
- w_output: bfloat16 [1024, 2048], P(None, 'tp'), may hold values from -0.1875 to 0.1875
- ffn_gain: float32 [2048], replicated, may hold values from 0.1 to 1.9
- expert_ids: int32 [256, 2], P('ep'), may hold values from 0 to 7, all different within a row; in each aligned block of 32 rows (0 to 31, 32 to 63, ...) at most 16 rows name the same one
- route_weight: float32 [256, 2], P('ep'), may hold values from 0.2 to 1
- expert_gate: bfloat16 [8, 2048, 3072], P('ep', None, 'tp'), may hold values from -0.125 to 0.125
- expert_up: bfloat16 [8, 2048, 3072], P('ep', None, 'tp'), may hold values from -0.125 to 0.125
- expert_down: bfloat16 [8, 3072, 2048], P('ep', 'tp'), may hold values from -0.109375 to 0.109375
- dense_gate: bfloat16 [2048, 4096], P(None, 'ep'), may hold values from -0.125 to 0.125
- dense_up: bfloat16 [2048, 4096], P(None, 'ep'), may hold values from -0.125 to 0.125
- dense_down: bfloat16 [4096, 2048], P('ep'), may hold values from -0.09375 to 0.09375
- dense_mix: float32 [2048], P('tp'), may hold values from -6 to 6
Outputs:
- result: bfloat16 [256, 2048], P('ep', 'tp')
- new_state: float32 [256, 8, 128, 128], P('ep', 'tp')
Inputs may be any that keep to these rules, and one draw needn't show every extreme that they name: `expert_ids`: each row names 2 different experts. Within the rows of one index of ep (aligned blocks of 32 sequences) no expert is named more than 16 times, a bound that some block reaches.
All inputs are finite; a program needn't handle non-finite values.
Results may differ from a plain program's by a relative error of at most 0.015.
Values may be sent and summed in bfloat16 or wider, within the bound.
No kernel may reach another device: no remote copies, remote signals or barrier semaphores. Data moves between devices by JAX's collectives and lax.ppermute only.
A program may use at most 64 MiB of HBM per device.

v0:
```python
import jax
import jax.numpy as jnp
from jax import lax
from jax.sharding import PartitionSpec as P

EPS = 1e-06


def root_norm(values, scale_vec):
    wide = values.astype(jnp.float32)
    return wide * lax.rsqrt(jnp.mean(wide * wide, axis=-1, keepdims=True) + EPS) * scale_vec


def unit_norm(values):
    return values * lax.rsqrt(jnp.sum(values * values, axis=-1, keepdims=True) + EPS)


def slot_table(expert_ids, count):
    flat = expert_ids.reshape(-1)
    onehot = (flat[:, None] == jnp.arange(count, dtype=jnp.int32)[None, :]).astype(jnp.int32)
    before = jnp.cumsum(onehot, axis=0) - onehot
    return jnp.sum(before * onehot, axis=1).reshape(expert_ids.shape)


def delta_update(old_state, key_rows, value_rows, beta_rate, decay_rate):
    recalled = jnp.einsum("shk,shkv->shv", key_rows, old_state, precision=lax.Precision.HIGHEST)
    erased = (
        old_state - beta_rate[..., None, None] * key_rows[..., :, None] * recalled[..., None, :]
    )
    written = beta_rate[..., None, None] * key_rows[..., :, None] * value_rows[..., None, :]
    return decay_rate[..., None, None] * erased + written


def head_output(new_state, queries, gate_rows, head_gain):
    read = jnp.einsum("shk,shkv->shv", queries, new_state, precision=lax.Precision.HIGHEST)
    return (root_norm(read, head_gain) * jax.nn.silu(gate_rows)).astype(jnp.bfloat16)


def per_device(
    hidden_in,
    state_in,
    attn_gain,
    w_query,
    w_key,
    w_value,
    w_gate,
    w_beta,
    w_decay,
    decay_scale,
    head_gain,
    w_output,
    ffn_gain,
    expert_ids,
    route_weight,
    expert_gate,
    expert_up,
    expert_down,
    dense_gate,
    dense_up,
    dense_down,
    dense_mix,
):
    seq_dev = hidden_in.shape[0]
    tp_size = lax.axis_size("tp")
    ep_size = lax.axis_size("ep")
    tp_index = lax.axis_index("tp")
    local_heads = state_in.shape[1]
    key_dim = state_in.shape[2]
    value_dim = state_in.shape[3]
    local_width = hidden_in.shape[1]
    model_width = local_width * tp_size
    full_rows = lax.all_gather(hidden_in, "tp", axis=1, tiled=True)
    normed = root_norm(full_rows, attn_gain).astype(jnp.bfloat16)
    queries = unit_norm(
        jnp.dot(normed, w_query, preferred_element_type=jnp.float32).reshape(
            seq_dev, local_heads, key_dim
        )
    ) * key_dim ** (-0.5)
    key_rows = unit_norm(
        jnp.dot(normed, w_key, preferred_element_type=jnp.float32).reshape(
            seq_dev, local_heads, key_dim
        )
    )
    value_rows = jnp.dot(normed, w_value, preferred_element_type=jnp.float32).reshape(
        seq_dev, local_heads, value_dim
    )
    gate_rows = jnp.dot(normed, w_gate, preferred_element_type=jnp.float32).reshape(
        seq_dev, local_heads, value_dim
    )
    head_start = tp_index * local_heads
    beta_all = jnp.dot(normed, w_beta, preferred_element_type=jnp.float32)
    decay_all = jnp.dot(normed, w_decay, preferred_element_type=jnp.float32)
    beta_rate = jax.nn.sigmoid(lax.dynamic_slice_in_dim(beta_all, head_start, local_heads, 1))
    decay_logit = lax.dynamic_slice_in_dim(decay_all, head_start, local_heads, 1)
    decay_local = lax.dynamic_slice_in_dim(decay_scale, head_start, local_heads, 0)
    decay_rate = jnp.exp(-decay_local[None, :] * jax.nn.softplus(decay_logit))
    new_state = delta_update(state_in, key_rows, value_rows, beta_rate, decay_rate)
    heads_out = head_output(new_state, queries, gate_rows, head_gain).reshape(
        seq_dev, local_heads * value_dim
    )
    all_heads = lax.all_gather(heads_out, "tp", axis=1, tiled=True)
    mixed = (
        hidden_in.astype(jnp.float32)
        + jnp.dot(all_heads, w_output, preferred_element_type=jnp.float32)
    ).astype(jnp.bfloat16)
    block_rows = seq_dev // tp_size
    top_count = expert_ids.shape[1]
    experts_all = expert_gate.shape[0] * ep_size
    capacity = max(2, 2 * seq_dev * top_count // experts_all)
    slots = slot_table(expert_ids, experts_all)
    place = expert_ids * capacity + slots
    columns = jnp.arange(experts_all * capacity, dtype=jnp.int32)
    send_matrix = jnp.sum(
        (place[None, :, :] == columns[:, None, None]).astype(jnp.bfloat16), axis=2
    )
    take_matrix = jnp.sum(
        jnp.where(place[:, :, None] == columns[None, None, :], route_weight[:, :, None], 0.0),
        axis=1,
    )
    mixed_full = lax.all_gather(mixed, "tp", axis=1, tiled=True)
    normed2 = root_norm(mixed_full, ffn_gain).astype(jnp.bfloat16)
    dense_rows = lax.dynamic_slice_in_dim(normed2, tp_index * block_rows, block_rows, 0)
    outgoing = jnp.dot(send_matrix, normed2, preferred_element_type=jnp.float32).astype(
        jnp.bfloat16
    )
    outgoing = outgoing.reshape(experts_all, capacity, model_width)
    rows = lax.all_to_all(outgoing, "ep", split_axis=0, concat_axis=0, tiled=True)
    flat = rows.reshape(-1, rows.shape[2])
    gate_val = jnp.dot(flat, expert_gate[0], preferred_element_type=jnp.float32)
    up_val = jnp.dot(flat, expert_up[0], preferred_element_type=jnp.float32)
    inner = (jax.nn.silu(gate_val) * up_val).astype(jnp.bfloat16)
    partial_out = jnp.dot(inner, expert_down[0], preferred_element_type=jnp.float32).reshape(
        rows.shape
    )
    summed = lax.psum_scatter(
        partial_out.astype(jnp.bfloat16), "tp", scatter_dimension=2, tiled=True
    )
    returned = lax.all_to_all(summed, "ep", split_axis=0, concat_axis=0, tiled=True)
    moe_sum = jnp.dot(
        take_matrix,
        returned.reshape(-1, local_width).astype(jnp.float32),
        precision=lax.Precision.HIGHEST,
    )
    piece = lax.all_gather(dense_rows, "ep", axis=0, tiled=True)
    gate_val = jnp.dot(piece, dense_gate, preferred_element_type=jnp.float32)
    up_val = jnp.dot(piece, dense_up, preferred_element_type=jnp.float32)
    dense_hidden = (jax.nn.silu(gate_val) * up_val).astype(jnp.bfloat16)
    dense_own = lax.psum_scatter(
        jnp.dot(dense_hidden, dense_down, preferred_element_type=jnp.float32).astype(jnp.bfloat16),
        "ep",
        scatter_dimension=0,
        tiled=True,
    ).astype(jnp.float32)
    dense_out = lax.all_to_all(
        dense_own.astype(jnp.bfloat16), "tp", split_axis=1, concat_axis=0, tiled=True
    ).astype(dense_own.dtype)
    result = (
        mixed.astype(jnp.float32) + moe_sum + jax.nn.sigmoid(dense_mix)[None, :] * dense_out
    ).astype(jnp.bfloat16)
    return (result, new_state)


def solution(mesh):
    placed = (
        P("ep", "tp"),
        P("ep", "tp", None, None),
        P(),
        P(None, "tp"),
        P(None, "tp"),
        P(None, "tp"),
        P(None, "tp"),
        P(),
        P(),
        P(),
        P(),
        P(None, "tp"),
        P(),
        P("ep", None),
        P("ep", None),
        P("ep", None, "tp"),
        P("ep", None, "tp"),
        P("ep", "tp", None),
        P(None, "ep"),
        P(None, "ep"),
        P("ep", None),
        P("tp"),
    )
    return jax.shard_map(
        per_device,
        mesh=mesh,
        in_specs=placed,
        out_specs=(P("ep", "tp"), P("ep", "tp", None, None)),
        check_vma=False,
    )
```

profile of v0, /device:TPU:0, one launch (start us, length us, event | category | flops | bytes accessed | tf_op | source)
XLA Modules:
  0.0 204.3 jit_solution(7041996628087368338)
XLA Ops:
  7.2 6.9 %all_gather.12 = bf16[32,2048]{1,0:T(8,128)(2,1)S(1)} all-gather(bf16[32,512]{1,0:T(8,128)(2,1)} %param.22), channel_id=1, replica_groups=mesh['ep'=8,'tp'=4] {'tp'}, dimensions={1}, use_global_device_ids=true | all-gather | bytes 163840 | tf_op jit(solution)/shard_map/all_gather | solution.py:72
  14.2 1.0 fusion.45
  15.2 1.0 fusion.47
  16.2 0.7 dynamic-slice_negate_fusion
  17.1 1.6 fusion.43
  18.9 1.6 fusion.41
  20.5 1.5 fusion.49
  22.5 5.5 %fusion.51 = f32[32,2,1,128]{3,2,1,0:T(1,128)S(1)} fusion(f32[32,2,128,1]{2,3,1,0:T(1,128)S(1)} %bitcast.72, f32[32,2,128,128]{3,2,1,0:T(8,128)} %param.23), kind=kOutput, calls=%fused_computation.74 | convolution fusion | flops 12582912 | bytes 4259840 | tf_op jit(solution)/shard_map/shk,shkv->shv/dot_general | solution.py:26
  28.0 1.5 multiply_add_fusion
  29.6 2.0 copy-done.2
  31.5 3.6 %fusion.52 = f32[32,2,1,128]{3,2,1,0:T(1,128)S(1)} fusion(f32[32,2,128,1]{2,3,1,0:T(1,128)S(1)} %bitcast.71, f32[32,2,128,128]{3,2,1,0:T(8,128)S(1)} %multiply_add_fusion), kind=kOutput, calls=%fused_computation.75 | convolution fusion | flops 12582912 | bytes 4259840 | tf_op jit(solution)/shard_map/shk,shkv->shv/dot_general | solution.py:35
  35.3 0.3 fusion.39
  35.8 5.4 %all_gather.13 = bf16[32,1024]{1,0:T(8,128)(2,1)S(1)} all-gather(bf16[32,256]{1,0:T(8,128)(2,1)S(1)} %bitcast.73), channel_id=1, replica_groups=mesh['ep'=8,'tp'=4] {'tp'}, dimensions={1}, use_global_device_ids=true | all-gather | bytes 81920 | tf_op jit(solution)/shard_map/all_gather | solution.py:101
  41.3 1.5 fusion.17
  42.8 0.6 copy-done.4
  43.4 5.4 %all_gather.14 = bf16[32,2048]{1,0:T(8,128)(2,1)S(1)} all-gather(bf16[32,512]{1,0:T(8,128)(2,1)S(1)} %fusion.17), channel_id=1, replica_groups=mesh['ep'=8,'tp'=4] {'tp'}, dimensions={1}, use_global_device_ids=true | all-gather | bytes 163840 | tf_op jit(solution)/shard_map/all_gather | solution.py:120
  49.3 0.2 select_reduce_fusion.1
  49.9 1.1 convolution_convert_fusion
  51.0 6.0 %all-to-all-start = ((bf16[8,16,2048]{2,1,0:T(8,128)(2,1)}), bf16[8,16,2048]{2,1,0:T(8,128)(2,1)}, u32[]{:S(2)}, u32[]{:S(2)}) async-start(bf16[8,16,2048]{2,1,0:T(8,128)(2,1)} %bitcast.65), calls=%async_computation | async-start | bytes 1048576 | tf_op jit(solution)/shard_map/all_to_all | solution.py:127
  57.1 38.0 %all_gather.15 = bf16[64,2048]{1,0:T(8,128)(2,1)S(1)} all-gather(bf16[8,2048]{1,0:T(8,128)(2,1)S(1)} %constant_dynamic-slice_fusion), channel_id=1, replica_groups=mesh['ep'=8,'tp'=4] {'ep'}, dimensions={0}, use_global_device_ids=true | all-gather | bytes 294912 | tf_op jit(solution)/shard_map/all_gather | solution.py:144
  95.0 2.1 %fusion.53 = f32[64,512]{1,0:T(8,128)S(1)} fusion(bf16[64,2048]{1,0:T(8,128)(2,1)S(1)} %all_gather.15, bf16[2048,512]{1,0:T(8,128)(2,1)} %param.40), kind=kOutput, calls=%fused_computation.76 | convolution fusion | flops 134217728 | bytes 2490368 | tf_op jit(solution)/shard_map/dot_general | solution.py:145
  97.1 3.9 %convolution_convert_fusion.1 = bf16[64,2048]{1,0:T(8,128)(2,1)} fusion(bf16[512,2048]{1,0:T(8,128)(2,1)} %param.42, bf16[64,2048]{1,0:T(8,128)(2,1)S(1)} %all_gather.15, bf16[2048,512]{1,0:T(8,128)(2,1)} %param.41, f32[64,512]{1,0:T(8,128)S(1)} %fusion.53), kind=kOutput, calls=%fused_computation.9 | convolution fusion | flops 268763136 | bytes 4849664 | tf_op jit(solution)/shard_map/dot_general | solution.py:149
  101.1 2.8 %fusion.4 = f32[128,768]{1,0:T(8,128)S(1)} fusion(bf16[128,2048]{1,0:T(8,128)(2,1)} %bitcast.9, bf16[1,2048,768]{2,1,0:T(8,128)(2,1)} %param.37), kind=kOutput, calls=%fused_computation.5 | convolution fusion | flops 402653184 | bytes 4063232 | tf_op jit(solution)/shard_map/dot_general | solution.py:129
  103.8 0.2 copy-done.13
  104.0 1.6 fusion.12
  105.7 1.4 fusion.6
  107.1 53.4 %reduce-scatter.5.cloned.1.call-done = bf16[8,2048]{1,0:T(8,128)(2,1)} async-done(((bf16[64,2048]{1,0:T(8,128)(2,1)}), bf16[8,2048]{1,0:T(8,128)(2,1)}) %reduce-scatter.5.cloned.1.call-update) | async-done | bytes 32784 | tf_op jit(solution)/shard_map/reduce_scatter | solution.py:148
  160.6 7.2 %all_to_all.23 = bf16[8,4,512]{2,0,1:T(8,128)(2,1)S(1)} all-to-all(bf16[8,4,512]{2,0,1:T(8,128)(2,1)} %bitcast.75), channel_id=1, replica_groups=mesh['ep'=8,'tp'=4] {'tp'}, dimensions={1} | all-to-all | bytes 65536 | tf_op jit(solution)/shard_map/all_to_all | solution.py:154
  167.7 16.1 %reduce-scatter.3.cloned.1.call-done = bf16[8,16,512]{2,1,0:T(8,128)(2,1)} async-done(((bf16[8,16,2048]{2,1,0:T(8,128)(2,1)}), bf16[8,16,512]{2,1,0:T(8,128)(2,1)}) %reduce-scatter.3.cloned.1.call-update) | async-done | bytes 131088 | tf_op jit(solution)/shard_map/reduce_scatter | solution.py:135
  183.8 5.5 %all-to-all-start.1 = ((bf16[8,16,512]{2,1,0:T(8,128)(2,1)}), bf16[8,16,512]{2,1,0:T(8,128)(2,1)S(1)}, u32[]{:S(2)}, u32[]{:S(2)}) async-start(bf16[8,16,512]{2,1,0:T(8,128)(2,1)} %reduce-scatter.3.cloned.1.call-done), calls=%async_computation.2 | async-start | bytes 262144 | tf_op jit(solution)/shard_map/all_to_all | solution.py:138
  189.5 7.2 %all-to-all-done.1 = bf16[8,16,512]{2,1,0:T(8,128)(2,1)S(1)} async-done(((bf16[8,16,512]{2,1,0:T(8,128)(2,1)}), bf16[8,16,512]{2,1,0:T(8,128)(2,1)S(1)}, u32[]{:S(2)}, u32[]{:S(2)}) %all-to-all-start.1) | async-done | bytes 131104 | tf_op jit(solution)/shard_map/all_to_all | solution.py:138
  196.7 0.8 fusion.18
  (63 shorter events, 2.3 us)
Async XLA Ops:
  7.2 98.6 %copy-start = (bf16[1,768,2048]{2,1,0:T(8,128)(2,1)S(1)}, bf16[1,768,2048]{2,1,0:T(8,128)(2,1)}, u32[]{:S(2)}) copy-start(bf16[1,768,2048]{2,1,0:T(8,128)(2,1)} %param.39) | copy-start | bytes 9437188
  7.2 13.3 %copy-start.6 = (f32[2048]{0:T(1024)S(1)}, f32[2048]{0:T(1024)}, u32[]{:S(2)}) copy-start(f32[2048]{0:T(1024)} %param.24) | copy-start | bytes 24580
  22.1 5.9 %copy-start.1 = (f32[32,2,128,128]{3,2,1,0:T(8,128)S(1)}, f32[32,2,128,128]{3,2,1,0:T(8,128)}, u32[]{:S(2)}) copy-start(f32[32,2,128,128]{3,2,1,0:T(8,128)} %param.23) | copy-start | bytes 12582916
  29.5 2.0 copy-start.2
  29.5 5.8 %copy-start.3 = (bf16[2048,256]{1,0:T(8,128)(2,1)S(1)}, bf16[2048,256]{1,0:T(8,128)(2,1)}, u32[]{:S(2)}) copy-start(bf16[2048,256]{1,0:T(8,128)(2,1)} %param.28) | copy-start | bytes 3145732
  29.6 6.2 %copy-start.12 = (f32[128]{0:T(128)S(1)}, f32[128]{0:T(128)}, u32[]{:S(2)}) copy-start(f32[128]{0:T(128)} %param.32) | copy-start | bytes 1540
  29.6 11.7 %copy-start.7 = (bf16[32,512]{1,0:T(8,128)(2,1)S(1)}, bf16[32,512]{1,0:T(8,128)(2,1)}, u32[]{:S(2)}) copy-start(bf16[32,512]{1,0:T(8,128)(2,1)} %param.22) | copy-start | bytes 98308
  31.5 17.4 %copy-start.9 = (s32[32,2]{0,1:T(2,128)S(1)}, s32[32,2]{0,1:T(2,128)}, u32[]{:S(2)}) copy-start(s32[32,2]{0,1:T(2,128)} %param.35) | copy-start | bytes 772
  31.5 18.2 %copy-start.8 = (f32[2048]{0:T(1024)S(1)}, f32[2048]{0:T(1024)}, u32[]{:S(2)}) copy-start(f32[2048]{0:T(1024)} %param.34) | copy-start | bytes 24580
  42.8 0.6 copy-start.4
  51.0 50.0 %all-to-all-start = ((bf16[8,16,2048]{2,1,0:T(8,128)(2,1)}), bf16[8,16,2048]{2,1,0:T(8,128)(2,1)}, u32[]{:S(2)}, u32[]{:S(2)}) async-start(bf16[8,16,2048]{2,1,0:T(8,128)(2,1)} %bitcast.65), calls=%async_computation | async-start | bytes 1048576 | tf_op jit(solution)/shard_map/all_to_all | solution.py:127
  57.0 103.6 %reduce-scatter.5.cloned.1.call-start = ((), (), s32[]{:S(2)}) async-start(), calls=%async_computation.6 | async-start | bytes 294912 | tf_op jit(solution)/shard_map/reduce_scatter | solution.py:148
  101.0 82.8 %reduce-scatter.3.cloned.1.call-start = ((), (), s32[]{:S(2)}) async-start(), calls=%async_computation.5 | async-start | bytes 655360 | tf_op jit(solution)/shard_map/reduce_scatter | solution.py:135
  101.0 3.0 %copy-start.13 = (bf16[1,2048,768]{2,1,0:T(8,128)(2,1)S(1)}, bf16[1,2048,768]{2,1,0:T(8,128)(2,1)}, u32[]{:S(2)}) copy-start(bf16[1,2048,768]{2,1,0:T(8,128)(2,1)} %param.38) | copy-start | bytes 9437188
  105.7 83.7 %copy-start.11 = (f32[32,2]{0,1:T(2,128)S(1)}, f32[32,2]{0,1:T(2,128)}, u32[]{:S(2)}) copy-start(f32[32,2]{0,1:T(2,128)} %param.36) | copy-start | bytes 772
  105.7 83.7 %copy-start.10 = (f32[512]{0:T(512)S(1)}, f32[512]{0:T(512)}, u32[]{:S(2)}) copy-start(f32[512]{0:T(512)} %param.43) | copy-start | bytes 6148
  105.7 91.0 %copy-start.5 = (bf16[32,512]{1,0:T(8,128)(2,1)S(1)}, bf16[32,512]{1,0:T(8,128)(2,1)}, u32[]{:S(2)}) copy-start(bf16[32,512]{1,0:T(8,128)(2,1)} %copy-done.4) | copy-start | bytes 98308
  183.8 12.9 %all-to-all-start.1 = ((bf16[8,16,512]{2,1,0:T(8,128)(2,1)}), bf16[8,16,512]{2,1,0:T(8,128)(2,1)S(1)}, u32[]{:S(2)}, u32[]{:S(2)}) async-start(bf16[8,16,512]{2,1,0:T(8,128)(2,1)} %reduce-scatter.3.cloned.1.call-done), calls=%async_computation.2 | async-start | bytes 262144 | tf_op jit(solution)/shard_map/all_to_all | solution.py:138
Sparse Core Ops, SparseCore 0:
  101.1 59.4 reduce-scatter.4
  163.1 20.7 reduce-scatter.2
where the time goes:
time: 205 us; the launch traced here: 204 us
  waiting for transfers between devices  76.8 us (37%)
  blocking collectives  62.8 us (31%)
  matrix products  31.3 us (15%)
  between operations  14.4 us (7%)
  starting transfers between devices  11.6 us (6%)
  other arithmetic  3.93 us (2%)
  local copies, waits for them, and re-layouts  3.54 us (2%)
    reduce_scatter x1, waiting for transfers between devices, per_device(): lax.psum_scatter(jnp.dot(dense_hidden, dense_down, preferred_element_type...  53.4 us
    all_gather x1, blocking collectives, per_device(): piece = lax.all_gather(dense_rows, 'ep', axis=0, tiled=True)  38 us
    reduce_scatter x1, waiting for transfers between devices, per_device(): lax.psum_scatter(partial_out.astype(jnp.bfloat16), 'tp', scatter_dimensio...  16.1 us
    all_to_all x1, waiting for transfers between devices, per_device(): lax.all_to_all(summed, 'ep', split_axis=0, concat_axis=0, tiled=True)  7.23 us
    all_to_all x1, blocking collectives, per_device(): lax.all_to_all(dense_own.astype(jnp.bfloat16), 'tp', split_axis=1, concat...  7.17 us
    all_gather x1, blocking collectives, per_device(): full_rows = lax.all_gather(hidden_in, 'tp', axis=1, tiled=True)  6.88 us
    all_to_all x1, starting transfers between devices, per_device(): lax.all_to_all(outgoing, 'ep', split_axis=0, concat_axis=0, tiled=True)  5.98 us
    all_to_all x1, starting transfers between devices, per_device(): lax.all_to_all(summed, 'ep', split_axis=0, concat_axis=0, tiled=True)  5.53 us
  transfers between devices with their start and end apart: 4, of which 3 were waited for; matrix products, arithmetic and copies ran while one was open for 6% of the time, Pallas kernels for 0%

commit v1 on v0

--- a/solution.py
+++ b/solution.py
@@ -141,7 +141,12 @@
         returned.reshape(-1, local_width).astype(jnp.float32),
         precision=lax.Precision.HIGHEST,
     )
-    piece = lax.all_gather(dense_rows, "ep", axis=0, tiled=True)
+    ring = [dense_rows]
+    for hop in range(7):
+        ring.append(lax.ppermute(ring[-1], "ep", [(dev, (dev + 1) % 8) for dev in range(8)]))
+    piece = jnp.roll(
+        jnp.concatenate(ring[::-1], axis=0), (lax.axis_index("ep") + 1) * ring[0].shape[0], axis=0
+    )
     gate_val = jnp.dot(piece, dense_gate, preferred_element_type=jnp.float32)
     up_val = jnp.dot(piece, dense_up, preferred_element_type=jnp.float32)
     dense_hidden = (jax.nn.silu(gate_val) * up_val).astype(jnp.bfloat16)

time: 205 us -> 211 us (1.029)
  waiting for transfers between devices: 76.8 us -> 118 us
  blocking collectives: 62.8 us -> 24.9 us
    all_gather x1 -> x0, blocking collectives: 38 us -> none  [per_device(): piece = lax.all_gather(dense_rows, 'ep', axis=0, tiled=True)]
    ppermute x0 -> x7, waiting for transfers between devices: none -> 37.2 us  [per_device(): lax.ppermute(ring[-1], 'ep', [(dev, (dev + 1) % 8) for dev in range(8)])]
    all_to_all x1, waiting for transfers between devices: 0.01 us -> 3.18 us  [per_device(): lax.all_to_all(outgoing, 'ep', split_axis=0, concat_axis=0, tiled=True)]
  transfers between devices with their start and end apart: 4 -> 11, of which waited for: 3 -> 10; matrix products, arithmetic and copies ran while one was open for 6% -> 7% of each run, Pallas kernels for 0% -> 0%
where the time goes in v1:
time: 211 us; the launch traced here: 210 us
  waiting for transfers between devices  118 us (56%)
  matrix products  31.4 us (15%)
  blocking collectives  24.9 us (12%)
  between operations  14.5 us (7%)
  starting transfers between devices  13.3 us (6%)
  other arithmetic  3.91 us (2%)
  local copies, waits for them, and re-layouts  3.8 us (2%)
    reduce_scatter x1, waiting for transfers between devices, per_device(): lax.psum_scatter(jnp.dot(dense_hidden, dense_down, preferred_element_type...  54.5 us
    ppermute x7, waiting for transfers between devices, per_device(): lax.ppermute(ring[-1], 'ep', [(dev, (dev + 1) % 8) for dev in range(8)])  37.2 us
    reduce_scatter x1, waiting for transfers between devices, per_device(): lax.psum_scatter(partial_out.astype(jnp.bfloat16), 'tp', scatter_dimensio...  16 us
    all_to_all x1, waiting for transfers between devices, per_device(): lax.all_to_all(summed, 'ep', split_axis=0, concat_axis=0, tiled=True)  7.23 us
    all_to_all x1, blocking collectives, per_device(): lax.all_to_all(dense_own.astype(jnp.bfloat16), 'tp', split_axis=1, concat...  7.17 us
    all_gather x1, blocking collectives, per_device(): full_rows = lax.all_gather(hidden_in, 'tp', axis=1, tiled=True)  6.88 us
    all_to_all x1, starting transfers between devices, per_device(): lax.all_to_all(outgoing, 'ep', split_axis=0, concat_axis=0, tiled=True)  6 us
    all_to_all x1, starting transfers between devices, per_device(): lax.all_to_all(summed, 'ep', split_axis=0, concat_axis=0, tiled=True)  5.51 us
  transfers between devices with their start and end apart: 11, of which 10 were waited for; matrix products, arithmetic and copies ran while one was open for 7% of the time, Pallas kernels for 0%

profile of v1, /device:TPU:0, one launch (start us, length us, event | category | flops | bytes accessed | tf_op | source)
XLA Modules:
  0.0 209.9 jit_solution(724918988436289061)
XLA Ops:
  7.2 6.9 %all_gather.9 = bf16[32,2048]{1,0:T(8,128)(2,1)S(1)} all-gather(bf16[32,512]{1,0:T(8,128)(2,1)} %param.22), channel_id=1, replica_groups=mesh['ep'=8,'tp'=4] {'tp'}, dimensions={1}, use_global_device_ids=true | all-gather | bytes 163840 | tf_op jit(solution)/shard_map/all_gather | solution.py:72
  14.2 1.0 fusion.50
  17.1 1.6 fusion.48
  18.9 1.6 fusion.46
  20.5 1.5 fusion.54
  22.5 5.5 %fusion.56 = f32[32,2,1,128]{3,2,1,0:T(1,128)S(1)} fusion(f32[32,2,128,1]{2,3,1,0:T(1,128)S(1)} %bitcast.70, f32[32,2,128,128]{3,2,1,0:T(8,128)} %param.23), kind=kOutput, calls=%fused_computation.90 | convolution fusion | flops 12582912 | bytes 4259840 | tf_op jit(solution)/shard_map/shk,shkv->shv/dot_general | solution.py:26
  28.0 1.5 multiply_add_fusion
  29.6 2.0 copy-done.2
  31.5 3.6 %fusion.57 = f32[32,2,1,128]{3,2,1,0:T(1,128)S(1)} fusion(f32[32,2,128,1]{2,3,1,0:T(1,128)S(1)} %bitcast.69, f32[32,2,128,128]{3,2,1,0:T(8,128)S(1)} %multiply_add_fusion), kind=kOutput, calls=%fused_computation.91 | convolution fusion | flops 12582912 | bytes 4259840 | tf_op jit(solution)/shard_map/shk,shkv->shv/dot_general | solution.py:35
  35.8 5.4 %all_gather.10 = bf16[32,1024]{1,0:T(8,128)(2,1)S(1)} all-gather(bf16[32,256]{1,0:T(8,128)(2,1)S(1)} %bitcast.71), channel_id=1, replica_groups=mesh['ep'=8,'tp'=4] {'tp'}, dimensions={1}, use_global_device_ids=true | all-gather | bytes 81920 | tf_op jit(solution)/shard_map/all_gather | solution.py:101
  41.3 1.5 fusion.16
  42.8 5.4 %all_gather.11 = bf16[32,2048]{1,0:T(8,128)(2,1)S(1)} all-gather(bf16[32,512]{1,0:T(8,128)(2,1)S(1)} %fusion.16), channel_id=1, replica_groups=mesh['ep'=8,'tp'=4] {'tp'}, dimensions={1}, use_global_device_ids=true | all-gather | bytes 163840 | tf_op jit(solution)/shard_map/all_gather | solution.py:120
  48.4 1.7 collective-permute-start
  50.2 4.9 %collective-permute-done = bf16[8,2048]{1,0:T(8,128)(2,1)S(1)} collective-permute-done((bf16[8,2048]{1,0:T(8,128)(2,1)S(1)}, bf16[8,2048]{1,0:T(8,128)(2,1)S(1)}, u32[]{:S(2)}, u32[]{:S(2)}) %collective-permute-start) | collective-permute-done | bytes 32800 | tf_op jit(solution)/shard_map/ppermute | solution.py:146
  55.3 6.4 %collective-permute-done.1 = bf16[8,2048]{1,0:T(8,128)(2,1)S(1)} collective-permute-done((bf16[8,2048]{1,0:T(8,128)(2,1)S(1)}, bf16[8,2048]{1,0:T(8,128)(2,1)S(1)}, u32[]{:S(2)}, u32[]{:S(2)}) %collective-permute-start.1) | collective-permute-done | bytes 32800 | tf_op jit(solution)/shard_map/ppermute | solution.py:146
  61.9 6.4 %collective-permute-done.2 = bf16[8,2048]{1,0:T(8,128)(2,1)S(1)} collective-permute-done((bf16[8,2048]{1,0:T(8,128)(2,1)S(1)}, bf16[8,2048]{1,0:T(8,128)(2,1)S(1)}, u32[]{:S(2)}, u32[]{:S(2)}) %collective-permute-start.2) | collective-permute-done | bytes 32800 | tf_op jit(solution)/shard_map/ppermute | solution.py:146
  68.7 6.2 %collective-permute-done.3 = bf16[8,2048]{1,0:T(8,128)(2,1)S(1)} collective-permute-done((bf16[8,2048]{1,0:T(8,128)(2,1)S(1)}, bf16[8,2048]{1,0:T(8,128)(2,1)S(1)}, u32[]{:S(2)}, u32[]{:S(2)}) %collective-permute-start.3) | collective-permute-done | bytes 32800 | tf_op jit(solution)/shard_map/ppermute | solution.py:146
  75.0 6.6 %collective-permute-done.4 = bf16[8,2048]{1,0:T(8,128)(2,1)S(1)} collective-permute-done((bf16[8,2048]{1,0:T(8,128)(2,1)S(1)}, bf16[8,2048]{1,0:T(8,128)(2,1)S(1)}, u32[]{:S(2)}, u32[]{:S(2)}) %collective-permute-start.4) | collective-permute-done | bytes 32800 | tf_op jit(solution)/shard_map/ppermute | solution.py:146
  81.6 6.5 %collective-permute-done.5 = bf16[8,2048]{1,0:T(8,128)(2,1)S(1)} collective-permute-done((bf16[8,2048]{1,0:T(8,128)(2,1)S(1)}, bf16[8,2048]{1,0:T(8,128)(2,1)S(1)}, u32[]{:S(2)}, u32[]{:S(2)}) %collective-permute-start.5) | collective-permute-done | bytes 32800 | tf_op jit(solution)/shard_map/ppermute | solution.py:146
  88.2 1.1 convolution_convert_fusion
  89.3 6.0 %all-to-all-start = ((bf16[8,16,2048]{2,1,0:T(8,128)(2,1)}), bf16[8,16,2048]{2,1,0:T(8,128)(2,1)}, u32[]{:S(2)}, u32[]{:S(2)}) async-start(bf16[8,16,2048]{2,1,0:T(8,128)(2,1)} %bitcast.63), calls=%async_computation | async-start | bytes 1048576 | tf_op jit(solution)/shard_map/all_to_all | solution.py:127
  96.4 2.1 fusion.24
  98.5 4.0 %convolution_convert_fusion.1 = bf16[64,2048]{1,0:T(8,128)(2,1)} fusion(bf16[512,2048]{1,0:T(8,128)(2,1)} %param.42, f32[64,512]{1,0:T(8,128)S(1)} %fusion.24, bf16[2048,512]{1,0:T(8,128)(2,1)} %param.40, bf16[128,2048]{1,0:T(8,128)(2,1)} %copy-done.4, s32[]{:T(128)S(6)} %select_n.34), kind=kOutput, calls=%fused_computation.9 | convolution fusion | flops 268763136 | bytes 4849668 | tf_op jit(solution)/shard_map/dot_general | solution.py:154
  102.5 3.2 %all-to-all-done = bf16[8,16,2048]{2,1,0:T(8,128)(2,1)} async-done(((bf16[8,16,2048]{2,1,0:T(8,128)(2,1)}), bf16[8,16,2048]{2,1,0:T(8,128)(2,1)}, u32[]{:S(2)}, u32[]{:S(2)}) %all-to-all-start) | async-done | bytes 524320 | tf_op jit(solution)/shard_map/all_to_all | solution.py:127
  105.7 2.8 %fusion.4 = f32[128,768]{1,0:T(8,128)S(1)} fusion(bf16[128,2048]{1,0:T(8,128)(2,1)} %bitcast.9, bf16[1,2048,768]{2,1,0:T(8,128)(2,1)} %param.37), kind=kOutput, calls=%fused_computation.5 | convolution fusion | flops 402653184 | bytes 4063232 | tf_op jit(solution)/shard_map/dot_general | solution.py:129
  108.7 1.6 fusion.12
  110.4 1.4 fusion.6
  111.8 54.5 %reduce-scatter.5.cloned.1.call-done = bf16[8,2048]{1,0:T(8,128)(2,1)} async-done(((bf16[64,2048]{1,0:T(8,128)(2,1)}), bf16[8,2048]{1,0:T(8,128)(2,1)}) %reduce-scatter.5.cloned.1.call-update) | async-done | bytes 32784 | tf_op jit(solution)/shard_map/reduce_scatter | solution.py:153
  166.3 7.2 %all_to_all.23 = bf16[8,4,512]{2,0,1:T(8,128)(2,1)S(1)} all-to-all(bf16[8,4,512]{2,0,1:T(8,128)(2,1)} %bitcast.73), channel_id=1, replica_groups=mesh['ep'=8,'tp'=4] {'tp'}, dimensions={1} | all-to-all | bytes 65536 | tf_op jit(solution)/shard_map/all_to_all | solution.py:159
  173.4 16.0 %reduce-scatter.3.cloned.1.call-done = bf16[8,16,512]{2,1,0:T(8,128)(2,1)} async-done(((bf16[8,16,2048]{2,1,0:T(8,128)(2,1)}), bf16[8,16,512]{2,1,0:T(8,128)(2,1)}) %reduce-scatter.3.cloned.1.call-update) | async-done | bytes 131088 | tf_op jit(solution)/shard_map/reduce_scatter | solution.py:135
  189.4 5.5 %all-to-all-start.1 = ((bf16[8,16,512]{2,1,0:T(8,128)(2,1)}), bf16[8,16,512]{2,1,0:T(8,128)(2,1)S(1)}, u32[]{:S(2)}, u32[]{:S(2)}) async-start(bf16[8,16,512]{2,1,0:T(8,128)(2,1)} %reduce-scatter.3.cloned.1.call-done), calls=%async_computation.2 | async-start | bytes 262144 | tf_op jit(solution)/shard_map/all_to_all | solution.py:138
  195.1 7.2 %all-to-all-done.1 = bf16[8,16,512]{2,1,0:T(8,128)(2,1)S(1)} async-done(((bf16[8,16,512]{2,1,0:T(8,128)(2,1)}), bf16[8,16,512]{2,1,0:T(8,128)(2,1)S(1)}, u32[]{:S(2)}, u32[]{:S(2)}) %all-to-all-start.1) | async-done | bytes 131104 | tf_op jit(solution)/shard_map/all_to_all | solution.py:138
  (90 shorter events, 6.5 us)
Async XLA Ops:
  7.2 103.2 %copy-start = (bf16[1,768,2048]{2,1,0:T(8,128)(2,1)S(1)}, bf16[1,768,2048]{2,1,0:T(8,128)(2,1)}, u32[]{:S(2)}) copy-start(bf16[1,768,2048]{2,1,0:T(8,128)(2,1)} %param.39) | copy-start | bytes 9437188
  7.2 13.3 %copy-start.5 = (f32[2048]{0:T(1024)S(1)}, f32[2048]{0:T(1024)}, u32[]{:S(2)}) copy-start(f32[2048]{0:T(1024)} %param.24) | copy-start | bytes 24580
  22.1 5.9 %copy-start.1 = (f32[32,2,128,128]{3,2,1,0:T(8,128)S(1)}, f32[32,2,128,128]{3,2,1,0:T(8,128)}, u32[]{:S(2)}) copy-start(f32[32,2,128,128]{3,2,1,0:T(8,128)} %param.23) | copy-start | bytes 12582916
  29.5 2.0 copy-start.2
  29.5 5.8 %copy-start.3 = (bf16[2048,256]{1,0:T(8,128)(2,1)S(1)}, bf16[2048,256]{1,0:T(8,128)(2,1)}, u32[]{:S(2)}) copy-start(bf16[2048,256]{1,0:T(8,128)(2,1)} %param.28) | copy-start | bytes 3145732
  29.6 6.2 %copy-start.11 = (f32[128]{0:T(128)S(1)}, f32[128]{0:T(128)}, u32[]{:S(2)}) copy-start(f32[128]{0:T(128)} %param.32) | copy-start | bytes 1540
  29.6 11.7 %copy-start.6 = (bf16[32,512]{1,0:T(8,128)(2,1)S(1)}, bf16[32,512]{1,0:T(8,128)(2,1)}, u32[]{:S(2)}) copy-start(bf16[32,512]{1,0:T(8,128)(2,1)} %param.22) | copy-start | bytes 98308
  31.5 16.8 %copy-start.7 = (f32[2048]{0:T(1024)S(1)}, f32[2048]{0:T(1024)}, u32[]{:S(2)}) copy-start(f32[2048]{0:T(1024)} %param.34) | copy-start | bytes 24580
  31.5 23.6 %copy-start.8 = (s32[32,2]{0,1:T(2,128)S(1)}, s32[32,2]{0,1:T(2,128)}, u32[]{:S(2)}) copy-start(s32[32,2]{0,1:T(2,128)} %param.35) | copy-start | bytes 772
  48.4 6.7 %collective-permute-start = (bf16[8,2048]{1,0:T(8,128)(2,1)S(1)}, bf16[8,2048]{1,0:T(8,128)(2,1)S(1)}, u32[]{:S(2)}, u32[]{:S(2)}) collective-permute-start(bf16[8,2048]{1,0:T(8,128)(2,1)S(1)} %constant_dynamic-slice_fusion), channel_id=1, source_target_pairs={{0,4},{4,8},{8,12},{12,16},{16,20},{20,24},{24,28},{28,0},{1,5},{5... | collective-permute-start | bytes 98312 | tf_op jit(solution)/shard_map/ppermute | solution.py:146
  55.1 6.6 %collective-permute-start.1 = (bf16[8,2048]{1,0:T(8,128)(2,1)S(1)}, bf16[8,2048]{1,0:T(8,128)(2,1)S(1)}, u32[]{:S(2)}, u32[]{:S(2)}) collective-permute-start(bf16[8,2048]{1,0:T(8,128)(2,1)S(1)} %collective-permute-done), channel_id=1, source_target_pairs={{0,4},{4,8},{8,12},{12,16},{16,20},{20,24},{24,28},{28,0},{1,5},{5... | collective-permute-start | bytes 98312 | tf_op jit(solution)/shard_map/ppermute | solution.py:146
  61.7 6.6 %collective-permute-start.2 = (bf16[8,2048]{1,0:T(8,128)(2,1)S(1)}, bf16[8,2048]{1,0:T(8,128)(2,1)S(1)}, u32[]{:S(2)}, u32[]{:S(2)}) collective-permute-start(bf16[8,2048]{1,0:T(8,128)(2,1)S(1)} %collective-permute-done.1), channel_id=1, source_target_pairs={{0,4},{4,8},{8,12},{12,16},{16,20},{20,24},{24,28},{28,0},{1,5},{5... | collective-permute-start | bytes 98312 | tf_op jit(solution)/shard_map/ppermute | solution.py:146
  68.3 6.6 %collective-permute-start.3 = (bf16[8,2048]{1,0:T(8,128)(2,1)S(1)}, bf16[8,2048]{1,0:T(8,128)(2,1)S(1)}, u32[]{:S(2)}, u32[]{:S(2)}) collective-permute-start(bf16[8,2048]{1,0:T(8,128)(2,1)S(1)} %collective-permute-done.2), channel_id=1, source_target_pairs={{0,4},{4,8},{8,12},{12,16},{16,20},{20,24},{24,28},{28,0},{1,5},{5... | collective-permute-start | bytes 98312 | tf_op jit(solution)/shard_map/ppermute | solution.py:146
  74.9 6.6 %collective-permute-start.4 = (bf16[8,2048]{1,0:T(8,128)(2,1)S(1)}, bf16[8,2048]{1,0:T(8,128)(2,1)S(1)}, u32[]{:S(2)}, u32[]{:S(2)}) collective-permute-start(bf16[8,2048]{1,0:T(8,128)(2,1)S(1)} %collective-permute-done.3), channel_id=1, source_target_pairs={{0,4},{4,8},{8,12},{12,16},{16,20},{20,24},{24,28},{28,0},{1,5},{5... | collective-permute-start | bytes 98312 | tf_op jit(solution)/shard_map/ppermute | solution.py:146
  81.6 6.6 %collective-permute-start.5 = (bf16[8,2048]{1,0:T(8,128)(2,1)S(1)}, bf16[8,2048]{1,0:T(8,128)(2,1)S(1)}, u32[]{:S(2)}, u32[]{:S(2)}) collective-permute-start(bf16[8,2048]{1,0:T(8,128)(2,1)S(1)} %collective-permute-done.4), channel_id=1, source_target_pairs={{0,4},{4,8},{8,12},{12,16},{16,20},{20,24},{24,28},{28,0},{1,5},{5... | collective-permute-start | bytes 98312 | tf_op jit(solution)/shard_map/ppermute | solution.py:146
  88.2 7.2 %collective-permute-start.6 = (bf16[8,2048]{1,0:T(8,128)(2,1)S(1)}, bf16[8,2048]{1,0:T(8,128)(2,1)S(1)}, u32[]{:S(2)}, u32[]{:S(2)}) collective-permute-start(bf16[8,2048]{1,0:T(8,128)(2,1)S(1)} %collective-permute-done.5), channel_id=1, source_target_pairs={{0,4},{4,8},{8,12},{12,16},{16,20},{20,24},{24,28},{28,0},{1,5},{5... | collective-permute-start | bytes 98312 | tf_op jit(solution)/shard_map/ppermute | solution.py:146
  89.3 16.4 %all-to-all-start = ((bf16[8,16,2048]{2,1,0:T(8,128)(2,1)}), bf16[8,16,2048]{2,1,0:T(8,128)(2,1)}, u32[]{:S(2)}, u32[]{:S(2)}) async-start(bf16[8,16,2048]{2,1,0:T(8,128)(2,1)} %bitcast.63), calls=%async_computation | async-start | bytes 1048576 | tf_op jit(solution)/shard_map/all_to_all | solution.py:127
  95.3 71.0 %reduce-scatter.5.cloned.1.call-start = ((), (), s32[]{:S(2)}) async-start(), calls=%async_computation.6 | async-start | bytes 294912 | tf_op jit(solution)/shard_map/reduce_scatter | solution.py:153
  95.6 0.8 copy-start.4
  102.5 87.0 %reduce-scatter.3.cloned.1.call-start = ((), (), s32[]{:S(2)}) async-start(), calls=%async_computation.5 | async-start | bytes 655360 | tf_op jit(solution)/shard_map/reduce_scatter | solution.py:135
  105.7 3.0 %copy-start.12 = (bf16[1,2048,768]{2,1,0:T(8,128)(2,1)S(1)}, bf16[1,2048,768]{2,1,0:T(8,128)(2,1)}, u32[]{:S(2)}) copy-start(bf16[1,2048,768]{2,1,0:T(8,128)(2,1)} %param.38) | copy-start | bytes 9437188
  110.3 84.6 %copy-start.10 = (f32[32,2]{0,1:T(2,128)S(1)}, f32[32,2]{0,1:T(2,128)}, u32[]{:S(2)}) copy-start(f32[32,2]{0,1:T(2,128)} %param.36) | copy-start | bytes 772
  110.3 84.7 %copy-start.9 = (f32[512]{0:T(512)S(1)}, f32[512]{0:T(512)}, u32[]{:S(2)}) copy-start(f32[512]{0:T(512)} %param.43) | copy-start | bytes 6148
  189.4 12.9 %all-to-all-start.1 = ((bf16[8,16,512]{2,1,0:T(8,128)(2,1)}), bf16[8,16,512]{2,1,0:T(8,128)(2,1)S(1)}, u32[]{:S(2)}, u32[]{:S(2)}) async-start(bf16[8,16,512]{2,1,0:T(8,128)(2,1)} %reduce-scatter.3.cloned.1.call-done), calls=%async_computation.2 | async-start | bytes 262144 | tf_op jit(solution)/shard_map/all_to_all | solution.py:138
Sparse Core Ops, SparseCore 0:
  102.6 63.6 reduce-scatter.4
  168.8 20.6 reduce-scatter.2
